TPU v7x, 512 devices: a whole 4x4x16 slice. The times are simulated.
512 devices in a mesh: sp: 16 (over y, x), tp: 32 (over z, core).
Axes of the slice: x: 4, y: 4, z: 16, core: 2. Of those that a mesh axis runs over, the one named last changes fastest.
Arguments:
- tokens: bfloat16 [32768, 2048], P('sp', 'tp'), may hold values from -6 to 6
- norm_gain: float32 [2048], replicated, may hold values from 0.1 to 1.9
- w_key: bfloat16 [2048, 1024], P(None, 'tp'), may hold values from -0.125 to 0.125
- w_decay: bfloat16 [2048, 1024], P(None, 'tp'), may hold values from -0.125 to 0.125
- w_value: bfloat16 [2048, 512], replicated, may hold values from -0.125 to 0.125
- decay_bias: float32 [1024], P('tp'), may hold values from 0 to 8.5
- gate_drift: float32 [32768], P('sp'), may hold values from -1 to 1
- queries: bfloat16 [1024], P('tp'), may hold values from -6 to 6
- out_gain: float32 [4, 512], P(None, 'sp'), may hold values from 0.1 to 1.9
Outputs:
- state_cache: bfloat16 [1024, 512], P('tp', 'sp')
- first_read: float32 [4, 512], P(None, 'sp')
All inputs are finite; a program needn't handle non-finite values.
Results may differ from a plain program's by a relative error of at most 0.009.
Values may be sent and summed in bfloat16 or wider, within the bound.
A program may use at most 128 MiB of HBM per device.

v0:
```python
import jax
import jax.numpy as jnp
from jax import lax
from jax.sharding import PartitionSpec as P

QUERY_KEY_HEADS = 4
KEY_CHANNELS = 256
VALUE_CHANNELS = 512
EPS = 1e-06
GATE_NORM = 16.0


def copy_for_each(shard, axis):
    copies = jnp.broadcast_to(shard, (lax.axis_size(axis), *shard.shape))
    return lax.all_to_all(copies, axis, split_axis=0, concat_axis=0, tiled=True)


def taken_together(shard, axis):
    return copy_for_each(shard, axis).sum(axis=0)


def body(tokens, norm_gain, w_key, w_decay, w_value, decay_bias, gate_drift, queries, out_gain):
    gathered = lax.all_gather(tokens, "tp", axis=1, tiled=True)
    rows_f32 = gathered.astype(jnp.float32)
    inverse_rms = lax.rsqrt(jnp.mean(rows_f32 * rows_f32, axis=1, keepdims=True) + EPS)
    normed = (rows_f32 * inverse_rms * norm_gain[None, :]).astype(jnp.bfloat16)
    key_proj = jnp.dot(normed, w_key, preferred_element_type=jnp.float32).astype(jnp.bfloat16)
    gate_pre = jnp.dot(normed, w_decay, preferred_element_type=jnp.float32).astype(jnp.bfloat16)
    value_proj = jnp.dot(normed, w_value, preferred_element_type=jnp.float32).astype(jnp.bfloat16)
    log_decay = (
        jax.nn.log_sigmoid(gate_pre.astype(jnp.float32) + decay_bias[None, :] + gate_drift[:, None])
        / GATE_NORM
    )
    suffix = lax.cumsum(log_decay, axis=0, reverse=True)
    weighted = (key_proj.astype(jnp.float32) * jnp.exp(suffix - log_decay)).astype(jnp.bfloat16)
    partial_value = lax.dot_general(
        weighted, value_proj, (((0,), (0,)), ((), ())), preferred_element_type=jnp.float32
    )
    total_decay = suffix[0]
    channels = partial_value.shape[0]
    span_count = lax.axis_size("sp")
    spread = jnp.broadcast_to(total_decay[None, :, None], (1, channels, span_count))
    blocks, totals = (
        lax.all_to_all(partial_value[None], "sp", split_axis=2, concat_axis=0, tiled=True),
        lax.all_to_all(spread, "sp", split_axis=2, concat_axis=0, tiled=True),
    )
    later_sum = lax.cumsum(totals, axis=0, reverse=True) - totals
    matrix_state = jnp.sum(jnp.exp(later_sum) * blocks, axis=0)
    state_cache = matrix_state.astype(jnp.bfloat16)
    channel_ids = lax.axis_index("tp") * channels + jnp.arange(channels, dtype=jnp.int32)
    owners = (channel_ids // KEY_CHANNELS)[:, None] == jnp.arange(QUERY_KEY_HEADS, dtype=jnp.int32)[
        None, :
    ]
    query_of_head = jnp.where(
        owners, queries.astype(jnp.float32)[:, None] * KEY_CHANNELS ** (-0.5), 0.0
    )
    part_read = lax.dot_general(query_of_head, matrix_state, (((0,), (0,)), ((), ())))
    summed_read = taken_together(part_read, "tp")
    squares = taken_together(jnp.sum(summed_read * summed_read, axis=1), "sp")
    first_read = summed_read * lax.rsqrt(squares / VALUE_CHANNELS + EPS)[:, None] * out_gain
    return (state_cache, first_read)


def solution(mesh):
    return jax.shard_map(
        body,
        mesh=mesh,
        in_specs=(
            P("sp", "tp"),
            P(),
            P(None, "tp"),
            P(None, "tp"),
            P(),
            P("tp"),
            P("sp"),
            P("tp"),
            P(None, "sp"),
        ),
        out_specs=(P("tp", "sp"), P(None, "sp")),
        check_vma=False,
    )
```

profile of v0, /device:TPU:1, one launch (start us, length us, event | category | flops | bytes accessed | tf_op | source)
XLA Modules:
  0.0 233.4 jit_solution(4992811210441940215)
XLA Ops:
  7.2 0.0 copy-start
  7.2 0.0 copy-start.3
  7.2 0.0 all-gather.2.cloned.1.call-start
  7.2 0.7 all-gather.2.cloned.1.call-update
  7.9 0.7 convert_multiply_fusion.2
  8.6 86.0 %all-gather.2.cloned.1.call-done = bf16[2048,2048]{0,1:T(8,128)(2,1)} async-done(((bf16[2048,64]{0,1:T(8,128)(2,1)}), bf16[2048,2048]{0,1:T(8,128)(2,1)}) %all-gather.2.cloned.1.call-update) | async-done | bytes 8388624 | tf_op jit(solution)/shard_map/all_gather | solution.py:23
  94.6 5.1 %fusion = f32[2048]{0:T(1024)S(1)} fusion(bf16[2048,2048]{0,1:T(8,128)(2,1)} %all-gather.2.cloned.1.call-done), kind=kLoop, calls=%fused_computation.2 | loop fusion | flops 12580864 | bytes 8396800 | tf_op jit(solution)/shard_map/reduce_sum | solution.py:25
  99.7 0.0 copy-done.3
  99.7 0.0 copy-start.1
  99.8 0.0 copy-start.4
  99.8 0.0 copy-start.6
  99.8 8.6 %fusion.2 = bf16[2048,2048]{0,1:T(8,128)(2,1)} fusion(bf16[2048,2048]{0,1:T(8,128)(2,1)} %all-gather.2.cloned.1.call-done, f32[2048]{0:T(1024)S(1)} %copy-done.3, f32[2048]{0:T(1024)S(1)} %add_rsqrt_fusion), kind=kLoop, calls=%fused_computation.4 | loop fusion | flops 16777216 | bytes 16793600 | tf_op jit(solution)/shard_map/convert_element_type | solution.py:26
  108.4 0.0 copy-done.1
  108.4 0.0 copy-start.2
  108.4 5.0 %fusion.9 = f32[2048,32]{0,1:T(8,128)S(1)} fusion(bf16[2048,32]{0,1:T(8,128)(2,1)S(1)} %copy-done.1, bf16[2048,2048]{0,1:T(8,128)(2,1)} %fusion.2, f32[2048]{0:T(1024)S(1)} %copy-done.4, f32[32]{0:T(128)S(1)} %copy-done.6), kind=kOutput, calls=%fused_computation.14 | convolution fusion | flops 268763136 | bytes 8790144 | tf_op jit(solution)/shard_map/dot_general | solution.py:28
  113.4 0.2 fusion.13
  113.6 39.7 %reduce-window.6 = f32[32,16,128]{2,1,0:T(8,128)S(1)} reduce-window(f32[32,16,128]{2,1,0:T(8,128)S(1)} %bitcast.59, f32[]{:T(128)} %constant.32.clone.1), window={size=1x1x128 pad=0_0x0_0x0_127}, to_apply=%region_1.2 | reduce-window | flops 8323072 | bytes 524292 | tf_op jit(solution)/shard_map/reduce-window
  153.3 0.2 copy.32
  153.5 0.2 reduce-window.9
  153.7 0.1 slice.13
  153.8 0.1 broadcast_add_fusion
  153.9 0.1 copy.40
  154.0 0.0 copy-done.2
  154.0 5.0 %fusion.5 = bf16[2048,32]{0,1:T(8,128)(2,1)S(1)} fusion(bf16[2048,32]{0,1:T(8,128)(2,1)S(1)} %copy-done.2, bf16[2048,2048]{0,1:T(8,128)(2,1)} %fusion.2, f32[2048,32]{0,1:T(8,128)S(1)} %fusion.9, f32[4,8,16,128]{3,2,1,0:T(8,128)S(1)} %bitcast.56), kind=kOutput, calls=%fused_computation.9 | convolution fusion | flops 269287424 | bytes 9175040 | tf_op jit(solution)/shard_map/dot_general | solution.py:27
  159.0 0.1 slice_reduce_fusion
  159.2 0.6 broadcast_in_dim.37
  159.8 6.6 %all-to-all-start = ((f32[1,32,16]{1,0,2:T(1,128)}), f32[1,32,16]{1,0,2:T(1,128)S(1)}, u32[]{:S(2)}, u32[]{:S(2)}) async-start(f32[1,32,16]{1,0,2:T(1,128)} %broadcast_in_dim.37), calls=%async_computation | async-start | bytes 16384 | tf_op jit(solution)/shard_map/all_to_all | solution.py:45
  166.4 0.0 copy-start.5
  166.4 9.2 %fusion.10 = f32[32,512]{0,1:T(8,128)S(1)} fusion(bf16[2048,32]{0,1:T(8,128)(2,1)S(1)} %fusion.5, bf16[2048,2048]{0,1:T(8,128)(2,1)} %fusion.2, bf16[2048,512]{1,0:T(8,128)(2,1)S(1)} %copy-done), kind=kOutput, calls=%fused_computation.15 | convolution fusion | flops 4363124736 | bytes 10682368 | tf_op jit(solution)/shard_map/dot_general | solution.py:36
  175.7 0.5 broadcast.91
  176.2 1.3 reduce.3
  177.5 0.8 reshape.75
  178.3 0.0 all-to-all-done
  178.3 6.6 %all-to-all-start.1 = ((f32[16,1,1024]{2,1,0:T(1,128)}), f32[16,1,1024]{2,1,0:T(1,128)S(1)}, u32[]{:S(2)}, u32[]{:S(2)}) async-start(f32[16,1,1024]{2,1,0:T(1,128)} %reshape.75), calls=%async_computation.1 | async-start | bytes 131072 | tf_op jit(solution)/shard_map/all_to_all | solution.py:44
  185.0 6.5 %all-to-all-done.1 = f32[16,1,1024]{2,1,0:T(1,128)S(1)} async-done(((f32[16,1,1024]{2,1,0:T(1,128)}), f32[16,1,1024]{2,1,0:T(1,128)S(1)}, u32[]{:S(2)}, u32[]{:S(2)}) %all-to-all-start.1) | async-done | bytes 65568 | tf_op jit(solution)/shard_map/all_to_all | solution.py:44
  191.4 0.8 reduce.4
  192.2 0.4 reshape.76
  192.7 0.2 fusion.22
  193.0 0.1 reshape.77
  193.1 21.4 %all_to_all.44 = f32[32,1,128]{2,1,0:T(1,128)S(1)} all-to-all(f32[32,1,128]{2,1,0:T(1,128)S(1)} %reshape.77), channel_id=1, replica_groups=mesh['sp'=16,'tp'=32] {'tp'}, dimensions={0} | all-to-all | bytes 32768 | tf_op jit(solution)/shard_map/all_to_all | solution.py:15
  214.5 0.7 reduce.5
  215.2 0.1 reshape.78
  215.3 0.1 multiply_reduce_fusion.1
  215.4 0.6 broadcast_in_dim.42
  216.0 3.5 %all-to-all-start.3 = ((f32[16,1,4]{2,1,0:T(1,128)}), f32[16,1,4]{2,1,0:T(1,128)S(1)}, u32[]{:S(2)}, u32[]{:S(2)}) async-start(f32[16,1,4]{2,1,0:T(1,128)} %broadcast_in_dim.42), calls=%async_computation.3 | async-start | bytes 16384 | tf_op jit(solution)/shard_map/all_to_all | solution.py:15
  219.5 0.7 copy.31
  220.2 5.7 %all-to-all-done.3 = f32[16,1,4]{2,1,0:T(1,128)S(1)} async-done(((f32[16,1,4]{2,1,0:T(1,128)}), f32[16,1,4]{2,1,0:T(1,128)S(1)}, u32[]{:S(2)}, u32[]{:S(2)}) %all-to-all-start.3) | async-done | bytes 288 | tf_op jit(solution)/shard_map/all_to_all | solution.py:15
  225.9 0.7 multiply_multiply_fusion
  (14 shorter events, 0.3 us)
Async XLA Ops:
  7.2 159.2 %copy-start = (bf16[2048,512]{1,0:T(8,128)(2,1)S(1)}, bf16[2048,512]{1,0:T(8,128)(2,1)}, u32[]{:S(2)}) copy-start(bf16[2048,512]{1,0:T(8,128)(2,1)} %param.13) | copy-start | bytes 6291460
  7.2 92.6 %copy-start.3 = (f32[2048]{0:T(1024)S(1)}, f32[2048]{0:T(1024)}, u32[]{:S(2)}) copy-start(f32[2048]{0:T(1024)} %param.10) | copy-start | bytes 24580
  7.2 87.4 %all-gather.2.cloned.1.call-start = ((), (), s32[]{:S(2)}) async-start(), calls=%async_computation.4 | async-start | bytes 8650752 | tf_op jit(solution)/shard_map/all_gather | solution.py:23
  99.7 8.6 %copy-start.1 = (bf16[2048,32]{0,1:T(8,128)(2,1)S(1)}, bf16[2048,32]{0,1:T(8,128)(2,1)}, u32[]{:S(2)}) copy-start(bf16[2048,32]{0,1:T(8,128)(2,1)} %param.12) | copy-start | bytes 393220
  99.8 8.6 %copy-start.4 = (f32[2048]{0:T(1024)S(1)}, f32[2048]{0:T(1024)}, u32[]{:S(2)}) copy-start(f32[2048]{0:T(1024)} %param.15) | copy-start | bytes 24580
  99.8 8.6 %copy-start.6 = (f32[32]{0:T(128)S(1)}, f32[32]{0:T(128)}, u32[]{:S(2)}) copy-start(f32[32]{0:T(128)} %param.14) | copy-start | bytes 388
  108.4 45.6 %copy-start.2 = (bf16[2048,32]{0,1:T(8,128)(2,1)S(1)}, bf16[2048,32]{0,1:T(8,128)(2,1)}, u32[]{:S(2)}) copy-start(bf16[2048,32]{0,1:T(8,128)(2,1)} %param.11) | copy-start | bytes 393220
  159.8 18.5 %all-to-all-start = ((f32[1,32,16]{1,0,2:T(1,128)}), f32[1,32,16]{1,0,2:T(1,128)S(1)}, u32[]{:S(2)}, u32[]{:S(2)}) async-start(f32[1,32,16]{1,0,2:T(1,128)} %broadcast_in_dim.37), calls=%async_computation | async-start | bytes 16384 | tf_op jit(solution)/shard_map/all_to_all | solution.py:45
  166.4 59.5 %copy-start.5 = (f32[4,32]{1,0:T(4,128)S(1)}, f32[4,32]{1,0:T(4,128)}, u32[]{:S(2)}) copy-start(f32[4,32]{1,0:T(4,128)} %param.17) | copy-start | bytes 1540
  178.3 13.2 %all-to-all-start.1 = ((f32[16,1,1024]{2,1,0:T(1,128)}), f32[16,1,1024]{2,1,0:T(1,128)S(1)}, u32[]{:S(2)}, u32[]{:S(2)}) async-start(f32[16,1,1024]{2,1,0:T(1,128)} %reshape.75), calls=%async_computation.1 | async-start | bytes 131072 | tf_op jit(solution)/shard_map/all_to_all | solution.py:44
  216.0 9.9 %all-to-all-start.3 = ((f32[16,1,4]{2,1,0:T(1,128)}), f32[16,1,4]{2,1,0:T(1,128)S(1)}, u32[]{:S(2)}, u32[]{:S(2)}) async-start(f32[16,1,4]{2,1,0:T(1,128)} %broadcast_in_dim.42), calls=%async_computation.3 | async-start | bytes 16384 | tf_op jit(solution)/shard_map/all_to_all | solution.py:15
Sparse Core Ops, SparseCore 0:
  10.1 84.4 all-gather.1
where the time goes:
time: 234 us; the launch traced here: 233 us
  waiting for transfers between devices  98.8 us (42%)
  other arithmetic  58.3 us (25%)
  blocking collectives  21.4 us (9%)
  matrix products  19.5 us (8%)
  starting transfers between devices  16.8 us (7%)
  between operations  14.3 us (6%)
  local copies, waits for them, and re-layouts  4.45 us (2%)
    all_gather x1, waiting for transfers between devices, body(): gathered = lax.all_gather(tokens, 'tp', axis=1, tiled=True)  86 us
    another operation x2, other arithmetic  39.9 us
    all_to_all x1, blocking collectives, copy_for_each(): return lax.all_to_all(copies, axis, split_axis=0, concat_axis=0, tiled=True)  21.4 us
    dot_general x1, matrix products, body(): lax.dot_general(weighted, value_proj, (((0,), (0,)), ((), ())), preferred...  9.21 us
    convert_element_type x1, other arithmetic, body(): normed = (rows_f32 * inverse_rms * norm_gain[None, :]).astype(jnp.bfloat16)  8.58 us
    all_to_all x1, starting transfers between devices, body(): lax.all_to_all(partial_value[None], 'sp', split_axis=2, concat_axis=0, ti...  6.65 us
    all_to_all x1, starting transfers between devices, body(): lax.all_to_all(spread, 'sp', split_axis=2, concat_axis=0, tiled=True)  6.63 us
    all_to_all x1, waiting for transfers between devices, body(): lax.all_to_all(partial_value[None], 'sp', split_axis=2, concat_axis=0, ti...  6.47 us
  transfers between devices with their start and end apart: 4, of which 3 were waited for; matrix products, arithmetic and copies ran while one was open for 6% of the time, Pallas kernels for 0%

commit v1 on v0

--- a/solution.py
+++ b/solution.py
@@ -20,7 +20,9 @@
 
 
 def body(tokens, norm_gain, w_key, w_decay, w_value, decay_bias, gate_drift, queries, out_gain):
-    gathered = lax.all_gather(tokens, "tp", axis=1, tiled=True)
+    gathered = jnp.concatenate(
+        lax.all_to_all(jnp.stack([tokens] * lax.axis_size("tp")), "tp", 0, 0), axis=1
+    )
     rows_f32 = gathered.astype(jnp.float32)
     inverse_rms = lax.rsqrt(jnp.mean(rows_f32 * rows_f32, axis=1, keepdims=True) + EPS)
     normed = (rows_f32 * inverse_rms * norm_gain[None, :]).astype(jnp.bfloat16)

time: 234 us -> 521 us (2.23)
  waiting for transfers between devices: 98.8 us -> 373 us
  starting transfers between devices: 16.8 us -> 33.8 us
  between operations: 14.3 us -> 0.89 us
  local copies, waits for them, and re-layouts: 4.45 us -> 9.83 us
    all_to_all x0 -> x1, waiting for transfers between devices: none -> 361 us  [body(): lax.all_to_all(jnp.stack([tokens] * lax.axis_size('tp')), 'tp', 0, 0)]
    all_gather x1 -> x0, waiting for transfers between devices: 86 us -> none  [body(): gathered = lax.all_gather(tokens, 'tp', axis=1, tiled=True)]
    all_to_all x0 -> x1, starting transfers between devices: none -> 16.9 us  [body(): lax.all_to_all(jnp.stack([tokens] * lax.axis_size('tp')), 'tp', 0, 0)]
    another operation x2 -> x3, local copies, waits for them, and re-layouts: 0.31 us -> 5.68 us  [the longest x1 5.37 us: body(): jnp.stack([tokens] * lax.axis_size('tp'))]
  transfers between devices with their start and end apart: 4 -> 4, of which waited for: 3 -> 3; matrix products, arithmetic and copies ran while one was open for 6% -> 2% of each run, Pallas kernels for 0% -> 0%
where the time goes in v1:
time: 521 us
  waiting for transfers between devices  373 us (72%)
  other arithmetic  57.6 us (11%)
  starting transfers between devices  33.8 us (6%)
  blocking collectives  26.4 us (5%)
  matrix products  19.5 us (4%)
  local copies, waits for them, and re-layouts  9.83 us (2%)
    all_to_all x1, waiting for transfers between devices, body(): lax.all_to_all(jnp.stack([tokens] * lax.axis_size('tp')), 'tp', 0, 0)  361 us
    another operation x2, other arithmetic  39.9 us
    all_to_all x1, blocking collectives, copy_for_each(): return lax.all_to_all(copies, axis, split_axis=0, concat_axis=0, tiled=True)  26.4 us
    all_to_all x1, starting transfers between devices, body(): lax.all_to_all(jnp.stack([tokens] * lax.axis_size('tp')), 'tp', 0, 0)  16.9 us
  transfers between devices with their start and end apart: 4, of which 3 were waited for; matrix products, arithmetic and copies ran while one was open for 2% of the time, Pallas kernels for 0%

profile of v1, /device:TPU:1, one launch (start us, length us, event | category | flops | bytes accessed | tf_op | source)
XLA Modules:
  0.0 520.7 jit_solution(2359272221282271251)
XLA Ops:
  0.6 0.0 copy-start
  0.6 5.4 %stack.2 = bf16[32,2048,64]{1,2,0:T(8,128)(2,1)} broadcast(bf16[2048,64]{0,1:T(8,128)(2,1)} %param.9), dimensions={1,2} | broadcast | bytes 8650752 | tf_op jit(solution)/shard_map/stack | solution.py:24
  6.0 16.9 %all-to-all-start = ((bf16[32,2048,64]{1,2,0:T(8,128)(2,1)}), bf16[32,2048,64]{1,2,0:T(8,128)(2,1)}, u32[]{:S(2)}, u32[]{:S(2)}) async-start(bf16[32,2048,64]{1,2,0:T(8,128)(2,1)} %stack.2), calls=%async_computation | async-start | bytes 16777216 | tf_op jit(solution)/shard_map/all_to_all | solution.py:24
  22.9 0.0 copy-start.3
  23.0 0.0 copy-done.7
  23.0 360.5 %all-to-all-done = bf16[32,2048,64]{1,2,0:T(8,128)(2,1)} async-done(((bf16[32,2048,64]{1,2,0:T(8,128)(2,1)}), bf16[32,2048,64]{1,2,0:T(8,128)(2,1)}, u32[]{:S(2)}, u32[]{:S(2)}) %all-to-all-start) | async-done | bytes 8388640 | tf_op jit(solution)/shard_map/all_to_all | solution.py:24
  383.5 5.1 multiply_reduce_fusion
  388.7 0.0 copy-done.3
  388.7 0.0 copy-start.1
  388.7 0.0 copy-start.4
  388.7 0.0 copy-start.6
  388.7 8.6 %fusion.1 = bf16[2048,2048]{0,1:T(8,128)(2,1)} fusion(f32[2048]{0:T(1024)S(1)} %copy-done.3, f32[2048]{0:T(1024)S(1)} %add_rsqrt_fusion, bf16[32,2048,64]{1,2,0:T(8,128)(2,1)} %all-to-all-done), kind=kLoop, calls=%fused_computation.2 | loop fusion | flops 16777216 | bytes 16793600 | tf_op jit(solution)/shard_map/convert_element_type | solution.py:28
  397.3 0.0 copy-done.4
  397.3 0.0 copy-start.2
  397.3 5.0 fusion.8
  402.3 0.2 fusion.12
  402.5 39.7 %reduce-window.6 = f32[32,16,128]{2,1,0:T(8,128)S(1)} reduce-window(f32[32,16,128]{2,1,0:T(8,128)S(1)} %bitcast.67, f32[]{:T(128)} %constant.32.clone.1), window={size=1x1x128 pad=0_0x0_0x0_127}, to_apply=%region_1.2 | reduce-window | flops 8323072 | bytes 524292 | tf_op jit(solution)/shard_map/reduce-window
  442.2 0.2 copy.33
  442.4 0.2 reduce-window.9
  442.6 0.1 slice.13
  442.7 0.1 broadcast_add_fusion
  442.8 0.1 copy.41
  442.9 5.0 fusion.4
  448.0 0.1 slice_reduce_fusion
  448.1 0.6 broadcast_in_dim.37
  448.7 6.8 %all-to-all-start.1 = ((f32[1,32,16]{1,0,2:T(1,128)}), f32[1,32,16]{1,0,2:T(1,128)S(1)}, u32[]{:S(2)}, u32[]{:S(2)}) async-start(f32[1,32,16]{1,0,2:T(1,128)} %broadcast_in_dim.37), calls=%async_computation.1 | async-start | bytes 16384 | tf_op jit(solution)/shard_map/all_to_all | solution.py:47
  455.5 0.0 copy-start.5
  455.5 9.2 %fusion.9 = f32[32,512]{0,1:T(8,128)S(1)} fusion(bf16[2048,32]{0,1:T(8,128)(2,1)S(1)} %fusion.4, bf16[2048,2048]{0,1:T(8,128)(2,1)} %fusion.1, bf16[2048,512]{1,0:T(8,128)(2,1)S(1)} %copy-done), kind=kOutput, calls=%fused_computation.14 | convolution fusion | flops 4363124736 | bytes 10682368 | tf_op jit(solution)/shard_map/dot_general | solution.py:38
  464.7 0.5 broadcast.93
  465.2 1.3 reduce.5
  466.5 0.8 reshape.82
  467.3 0.0 all-to-all-done.1
  467.3 6.6 %all-to-all-start.2 = ((f32[16,1,1024]{2,1,0:T(1,128)}), f32[16,1,1024]{2,1,0:T(1,128)S(1)}, u32[]{:S(2)}, u32[]{:S(2)}) async-start(f32[16,1,1024]{2,1,0:T(1,128)} %reshape.82), calls=%async_computation.2 | async-start | bytes 131072 | tf_op jit(solution)/shard_map/all_to_all | solution.py:46
  474.0 6.5 %all-to-all-done.2 = f32[16,1,1024]{2,1,0:T(1,128)S(1)} async-done(((f32[16,1,1024]{2,1,0:T(1,128)}), f32[16,1,1024]{2,1,0:T(1,128)S(1)}, u32[]{:S(2)}, u32[]{:S(2)}) %all-to-all-start.2) | async-done | bytes 65568 | tf_op jit(solution)/shard_map/all_to_all | solution.py:46
  480.5 0.8 reduce.6
  481.3 0.4 reshape.83
  481.8 0.2 fusion.21
  482.0 0.1 reshape.84
  482.2 26.4 %all_to_all.49 = f32[32,1,128]{2,1,0:T(1,128)S(1)} all-to-all(f32[32,1,128]{2,1,0:T(1,128)S(1)} %reshape.84), channel_id=1, replica_groups=mesh['sp'=16,'tp'=32] {'tp'}, dimensions={0} | all-to-all | bytes 32768 | tf_op jit(solution)/shard_map/all_to_all | solution.py:15
  508.6 0.7 reduce.7
  509.3 0.1 reshape.85
  509.4 0.1 multiply_reduce_fusion.2
  509.5 0.6 broadcast_in_dim.42
  510.1 3.5 all-to-all-start.4
  513.6 0.7 copy.32
  514.3 5.7 %all-to-all-done.4 = f32[16,1,4]{2,1,0:T(1,128)S(1)} async-done(((f32[16,1,4]{2,1,0:T(1,128)}), f32[16,1,4]{2,1,0:T(1,128)S(1)}, u32[]{:S(2)}, u32[]{:S(2)}) %all-to-all-start.4) | async-done | bytes 288 | tf_op jit(solution)/shard_map/all_to_all | solution.py:15
  520.0 0.0 copy-done.5
  520.0 0.7 multiply_multiply_fusion
  (16 shorter events, 0.3 us)
Async XLA Ops:
  0.6 454.8 %copy-start = (bf16[2048,512]{1,0:T(8,128)(2,1)S(1)}, bf16[2048,512]{1,0:T(8,128)(2,1)}, u32[]{:S(2)}) copy-start(bf16[2048,512]{1,0:T(8,128)(2,1)} %param.13) | copy-start | bytes 6291460
  6.0 17.0 %copy-start.7 = (bf16[32]{0:T(256)(128)(2,1)S(1)}, bf16[32]{0:T(256)(128)(2,1)}, u32[]{:S(2)}) copy-start(bf16[32]{0:T(256)(128)(2,1)} %param.16) | copy-start | bytes 196
  6.0 377.5 %all-to-all-start = ((bf16[32,2048,64]{1,2,0:T(8,128)(2,1)}), bf16[32,2048,64]{1,2,0:T(8,128)(2,1)}, u32[]{:S(2)}, u32[]{:S(2)}) async-start(bf16[32,2048,64]{1,2,0:T(8,128)(2,1)} %stack.2), calls=%async_computation | async-start | bytes 16777216 | tf_op jit(solution)/shard_map/all_to_all | solution.py:24
  22.9 365.7 %copy-start.3 = (f32[2048]{0:T(1024)S(1)}, f32[2048]{0:T(1024)}, u32[]{:S(2)}) copy-start(f32[2048]{0:T(1024)} %param.10) | copy-start | bytes 24580
  388.7 8.6 %copy-start.1 = (bf16[2048,32]{0,1:T(8,128)(2,1)S(1)}, bf16[2048,32]{0,1:T(8,128)(2,1)}, u32[]{:S(2)}) copy-start(bf16[2048,32]{0,1:T(8,128)(2,1)} %param.12) | copy-start | bytes 393220
  388.7 8.6 %copy-start.4 = (f32[2048]{0:T(1024)S(1)}, f32[2048]{0:T(1024)}, u32[]{:S(2)}) copy-start(f32[2048]{0:T(1024)} %param.15) | copy-start | bytes 24580
  388.7 8.6 %copy-start.6 = (f32[32]{0:T(128)S(1)}, f32[32]{0:T(128)}, u32[]{:S(2)}) copy-start(f32[32]{0:T(128)} %param.14) | copy-start | bytes 388
  397.3 45.6 %copy-start.2 = (bf16[2048,32]{0,1:T(8,128)(2,1)S(1)}, bf16[2048,32]{0,1:T(8,128)(2,1)}, u32[]{:S(2)}) copy-start(bf16[2048,32]{0,1:T(8,128)(2,1)} %param.11) | copy-start | bytes 393220
  448.7 18.6 %all-to-all-start.1 = ((f32[1,32,16]{1,0,2:T(1,128)}), f32[1,32,16]{1,0,2:T(1,128)S(1)}, u32[]{:S(2)}, u32[]{:S(2)}) async-start(f32[1,32,16]{1,0,2:T(1,128)} %broadcast_in_dim.37), calls=%async_computation.1 | async-start | bytes 16384 | tf_op jit(solution)/shard_map/all_to_all | solution.py:47
  455.5 64.6 %copy-start.5 = (f32[4,32]{1,0:T(4,128)S(1)}, f32[4,32]{1,0:T(4,128)}, u32[]{:S(2)}) copy-start(f32[4,32]{1,0:T(4,128)} %param.17) | copy-start | bytes 1540
  467.3 13.2 %all-to-all-start.2 = ((f32[16,1,1024]{2,1,0:T(1,128)}), f32[16,1,1024]{2,1,0:T(1,128)S(1)}, u32[]{:S(2)}, u32[]{:S(2)}) async-start(f32[16,1,1024]{2,1,0:T(1,128)} %reshape.82), calls=%async_computation.2 | async-start | bytes 131072 | tf_op jit(solution)/shard_map/all_to_all | solution.py:46
  510.1 9.9 %all-to-all-start.4 = ((f32[16,1,4]{2,1,0:T(1,128)}), f32[16,1,4]{2,1,0:T(1,128)S(1)}, u32[]{:S(2)}, u32[]{:S(2)}) async-start(f32[16,1,4]{2,1,0:T(1,128)} %broadcast_in_dim.42), calls=%async_computation.4 | async-start | bytes 16384 | tf_op jit(solution)/shard_map/all_to_all | solution.py:15
